TPU v7x, 32 devices: a whole 2x2x4 slice. The times are simulated.
32 devices in a mesh: fs: 8 (over z, y), tp: 4 (over x, core).
Axes of the slice: x: 2, y: 2, z: 4, core: 2. Of those that a mesh axis runs over, the one named last changes fastest.
Arguments:
- tokens: bfloat16 [8192, 2048], P('fs', 'tp'), may hold values from -6 to 6
- norm_gain: float32 [2048], P('fs'), may hold values from 0.1 to 1.9
- up_master: float32 [2048, 4096], P('fs', 'tp'), may hold values from -0.125 to 0.125
- down_master: float32 [4096, 2048], P('fs', 'tp'), may hold values from -0.09375 to 0.09375
Outputs:
- mixed: bfloat16 [8192, 2048], P('fs', 'tp')
- up_ready: bfloat16 [2048, 4096], P(None, 'tp')
- down_ready: bfloat16 [4096, 2048], P('tp')
All inputs are finite; a program needn't handle non-finite values.
Results may differ from a plain program's by a relative error of at most 0.0095.
Values may be sent and summed in bfloat16 or wider, within the bound.
A program may use at most 128 MiB of HBM per device.

v0:
```python
import jax
import jax.numpy as jnp
from jax import lax
from jax.sharding import PartitionSpec as P


def shards(tokens, norm_gain, up_master, down_master):
    up_local = (norm_gain[:, None] * up_master).astype(jnp.bfloat16)
    up_ready = lax.all_gather(up_local, "fs", axis=0, tiled=True)
    down_local = down_master.astype(jnp.bfloat16)
    gathered = lax.all_gather(down_local, "fs", axis=0, tiled=True)
    down_ready = lax.all_to_all(gathered, "tp", split_axis=0, concat_axis=1, tiled=True)
    features = lax.all_gather(tokens, "tp", axis=1, tiled=True)
    values = features.astype(jnp.float32)
    mean_square = jnp.mean(values * values, axis=-1, keepdims=True)
    normed = (values * lax.rsqrt(mean_square + 1e-06)).astype(jnp.bfloat16)
    before = jnp.dot(normed, up_ready, preferred_element_type=jnp.float32)
    hidden = jnp.square(jax.nn.relu(before)).astype(jnp.bfloat16)
    partial_value = jnp.dot(hidden, down_ready, preferred_element_type=jnp.float32)
    mixed = lax.psum_scatter(
        partial_value.astype(jnp.bfloat16), "tp", scatter_dimension=1, tiled=True
    )
    return (mixed, up_ready, down_ready)


def solution(mesh):
    return jax.shard_map(
        shards,
        mesh=mesh,
        in_specs=(P("fs", "tp"), P("fs"), P("fs", "tp"), P("fs", "tp")),
        out_specs=(P("fs", "tp"), P(None, "tp"), P("tp", None)),
        check_vma=False,
    )
```

profile of v0, /device:TPU:0, one launch (start us, length us, event | category | flops | bytes accessed | tf_op | source)
XLA Modules:
  0.0 287.9 jit_solution(17428654618168584598)
XLA Ops:
  7.2 0.0 all-gather.8.cloned.1.call-start
  7.2 2.1 convert_element_type.22
  9.3 0.0 all-gather.8.cloned.1.call-update
  9.3 0.0 all-gather.4.cloned.1.call-start
  9.4 0.7 all-gather.4.cloned.1.call-update
  10.1 0.0 all-gather.6.cloned.1.call-start
  10.1 2.1 multiply_convert_fusion.2
  12.3 0.0 all-gather.6.cloned.1.call-update
  12.3 73.9 %all-gather.8.cloned.1.call-done = bf16[4096,512]{1,0:T(8,128)(2,1)} async-done(((bf16[512,512]{1,0:T(8,128)(2,1)}), bf16[4096,512]{1,0:T(8,128)(2,1)}) %all-gather.8.cloned.1.call-update) | async-done | bytes 4194320 | tf_op jit(solution)/shard_map/all_gather | solution.py:11
  86.2 4.9 %all-to-all-start = ((bf16[4,1024,512]{2,1,0:T(8,128)(2,1)}), bf16[4,1024,512]{2,1,0:T(8,128)(2,1)}, u32[]{:S(2)}, u32[]{:S(2)}) async-start(bf16[4,1024,512]{2,1,0:T(8,128)(2,1)} %bitcast.8), calls=%async_computation | async-start | bytes 8388608 | tf_op jit(solution)/shard_map/all_to_all | solution.py:12
  91.1 0.0 reduce-scatter.2.cloned.1.call-start
  91.2 52.2 %all-gather.4.cloned.1.call-done = bf16[1024,2048]{1,0:T(8,128)(2,1)} async-done(((bf16[1024,512]{1,0:T(8,128)(2,1)}), bf16[1024,2048]{1,0:T(8,128)(2,1)}) %all-gather.4.cloned.1.call-update) | async-done | bytes 4194320 | tf_op jit(solution)/shard_map/all_gather | solution.py:13
  143.4 3.1 %fusion = f32[1024]{0:T(1024)S(1)} fusion(bf16[1024,2048]{1,0:T(8,128)(2,1)} %all-gather.4.cloned.1.call-done), kind=kLoop, calls=%fused_computation.2 | loop fusion | flops 6290432 | bytes 4198400 | tf_op jit(solution)/shard_map/reduce_sum | solution.py:15
  146.5 15.3 %all-to-all-done = bf16[4,1024,512]{2,1,0:T(8,128)(2,1)} async-done(((bf16[4,1024,512]{2,1,0:T(8,128)(2,1)}), bf16[4,1024,512]{2,1,0:T(8,128)(2,1)}, u32[]{:S(2)}, u32[]{:S(2)}) %all-to-all-start) | async-done | bytes 4194336 | tf_op jit(solution)/shard_map/all_to_all | solution.py:12
  161.8 6.2 %copy.8 = bf16[4,1024,512]{1,2,0:T(8,128)(2,1)} copy(bf16[4,1024,512]{2,1,0:T(8,128)(2,1)} %all-to-all-done) | data formatting | bytes 8388608 | tf_op jit(solution)/shard_map/all_to_all | solution.py:12
  168.0 50.9 %all-gather.6.cloned.1.call-done = bf16[2048,1024]{1,0:T(8,128)(2,1)} async-done(((bf16[256,1024]{1,0:T(8,128)(2,1)}), bf16[2048,1024]{1,0:T(8,128)(2,1)}) %all-gather.6.cloned.1.call-update) | async-done | bytes 4194320 | tf_op jit(solution)/shard_map/all_gather | solution.py:9
  218.9 14.7 %convolution_convert_fusion = bf16[1024,2048]{1,0:T(8,128)(2,1)} fusion(bf16[1024,2048]{0,1:T(8,128)(2,1)} %bitcast.6, bf16[2048,1024]{1,0:T(8,128)(2,1)} %all-gather.6.cloned.1.call-done, bf16[1024,2048]{1,0:T(8,128)(2,1)} %all-gather.4.cloned.1.call-done, f32[1024]{0:T(1024)S(1)} %add_rsqrt_fusion), kind=kOutput, calls=%fused_computation.7 | convolution fusion | flops 8601468928 | bytes 16781312 | tf_op jit(solution)/shard_map/dot_general | solution.py:19
  233.6 0.0 reduce-scatter.2.cloned.1.call-update
  233.6 6.5 %copy.9 = bf16[1024,2048]{1,0:T(8,128)(2,1)} copy(bf16[1024,2048]{0,1:T(8,128)(2,1)} %bitcast.7) | data formatting | bytes 8388608
  240.1 36.6 %reduce-scatter.2.cloned.1.call-done = bf16[1024,512]{1,0:T(8,128)(2,1)} async-done(((bf16[1024,2048]{1,0:T(8,128)(2,1)}), bf16[1024,512]{1,0:T(8,128)(2,1)}) %reduce-scatter.2.cloned.1.call-update) | async-done | bytes 1048592 | tf_op jit(solution)/shard_map/reduce_scatter | solution.py:20
  276.7 4.6 %copy.11 = bf16[2048,1024]{1,0:T(8,128)(2,1)} copy(bf16[2048,1024]{1,0:T(8,128)(2,1)} %all-gather.6.cloned.1.call-done) | data formatting | bytes 8388608
  (1 shorter events, 0.0 us)
Async XLA Ops:
  7.2 79.1 %all-gather.8.cloned.1.call-start = ((), (), s32[]{:S(2)}) async-start(), calls=%async_computation.4 | async-start | bytes 4718592 | tf_op jit(solution)/shard_map/all_gather | solution.py:11
  9.3 134.1 %all-gather.4.cloned.1.call-start = ((), (), s32[]{:S(2)}) async-start(), calls=%async_computation.2 | async-start | bytes 5242880 | tf_op jit(solution)/shard_map/all_gather | solution.py:13
  10.1 208.8 %all-gather.6.cloned.1.call-start = ((), (), s32[]{:S(2)}) async-start(), calls=%async_computation.3 | async-start | bytes 4718592 | tf_op jit(solution)/shard_map/all_gather | solution.py:9
  86.2 75.6 %all-to-all-start = ((bf16[4,1024,512]{2,1,0:T(8,128)(2,1)}), bf16[4,1024,512]{2,1,0:T(8,128)(2,1)}, u32[]{:S(2)}, u32[]{:S(2)}) async-start(bf16[4,1024,512]{2,1,0:T(8,128)(2,1)} %bitcast.8), calls=%async_computation | async-start | bytes 8388608 | tf_op jit(solution)/shard_map/all_to_all | solution.py:12
  91.1 185.6 %reduce-scatter.2.cloned.1.call-start = ((), (), s32[]{:S(2)}) async-start(), calls=%async_computation.5 | async-start | bytes 5242880 | tf_op jit(solution)/shard_map/reduce_scatter | solution.py:20
Sparse Core Ops, SparseCore 0:
  10.7 75.5 all-gather.7
  87.8 55.5 all-gather.3
  146.1 72.7 all-gather.5
  233.7 42.9 reduce-scatter.1
where the time goes:
time: 288 us
  waiting for transfers between devices  230 us (80%)
  local copies, waits for them, and re-layouts  17.3 us (6%)
  matrix products  14.7 us (5%)
  between operations  13.8 us (5%)
  other arithmetic  7.31 us (3%)
  starting transfers between devices  5.06 us (2%)
    all_gather x1, waiting for transfers between devices, shards(): gathered = lax.all_gather(down_local, 'fs', axis=0, tiled=True)  73.9 us
    all_gather x1, waiting for transfers between devices, shards(): features = lax.all_gather(tokens, 'tp', axis=1, tiled=True)  52.2 us
    all_gather x1, waiting for transfers between devices, shards(): up_ready = lax.all_gather(up_local, 'fs', axis=0, tiled=True)  50.9 us
    reduce_scatter x1, waiting for transfers between devices, shards(): lax.psum_scatter(partial_value.astype(jnp.bfloat16), 'tp', scatter_dimens...  36.6 us
    all_to_all x1, waiting for transfers between devices, shards(): lax.all_to_all(gathered, 'tp', split_axis=0, concat_axis=1, tiled=True)  15.3 us
    dot_general x1, matrix products, shards(): jnp.dot(hidden, down_ready, preferred_element_type=jnp.float32)  14.7 us
    unnamed x2, local copies, waits for them, and re-layouts  11.1 us
    all_to_all x1, local copies, waits for them, and re-layouts, shards(): lax.all_to_all(gathered, 'tp', split_axis=0, concat_axis=1, tiled=True)  6.21 us
  transfers between devices with their start and end apart: 5, of which 5 were waited for; matrix products, arithmetic and copies ran while one was open for 6% of the time, Pallas kernels for 0%

commit v1 on v0

v1 whole, which is shorter than its diff:
```python
import functools

import jax
import jax.numpy as jnp
from jax import lax
from jax.experimental import pallas as pl
from jax.experimental.pallas import tpu as pltpu
from jax.sharding import PartitionSpec as P

UP_CUTS = 2
DOWN_CUTS = 4
COLUMNS = 256
MIB = 1024 * 1024


def kernel(
    n, n_tp,
    tokens_ref, gain_ref, upm_ref, downm_ref,
    mixed_ref, upo_ref, downo_ref,
    tok, up, down, shard, scale, hidden, kept, give, take, cross, crossed, own,
    tok_send, tok_recv, gather_send, gather_recv,
    up_send, upz_recv, upy_recv,
    down_send, downz_recv, downy_recv,
    pair_send, pair_recv, cross_send, cross_recv, local_sem,
):
    f32, bf16 = jnp.float32, jnp.bfloat16
    f, t = lax.axis_index("fs"), lax.axis_index("tp")
    lines = n // 2
    z, y = f // 2, f % 2
    t1 = t + 1 - 2 * (t % 2)
    t2 = (t + 2) % 4
    t3 = (t1 + 2) % 4
    members = n // n_tp
    starts = members // 2
    owner = f // members
    above, below = (f + 2) % n, (f + n - 2) % n
    across = f + 1 - 2 * y
    has_above, has_below = z < lines - 1, z > 0

    up_rows = upm_ref.shape[0]
    down_rows = downm_ref.shape[0]
    feats = tokens_ref.shape[1]
    ucut, dcut = up_rows // UP_CUTS, down_rows // DOWN_CUTS

    def remote(src, dst, send, recv, **to):
        return pltpu.make_async_remote_copy(
            src_ref=src, dst_ref=dst, send_sem=send, recv_sem=recv,
            device_id=to, device_id_type=pl.DeviceIdType.MESH,
        )

    load = pltpu.make_async_copy(
        tokens_ref, tok.at[:, pl.ds(pl.multiple_of(t * feats, feats), feats)], local_sem.at[0]
    )
    load.start()

    shard[...] = downm_ref[...].astype(bf16)

    def down_block(source, column):
        rows = pl.ds(pl.multiple_of(source % members * down_rows, down_rows), down_rows)
        return down.at[rows, pl.ds(pl.multiple_of(column * feats, feats), feats)]

    @pl.when(owner == t)
    def _():
        down_block(f, t)[...] = downm_ref[...].astype(bf16)

    up[pl.ds(pl.multiple_of(f * up_rows, up_rows), up_rows), :] = (
        gain_ref[...] * upm_ref[...]
    ).astype(bf16)

    barrier = pltpu.get_barrier_semaphore()
    for other in (t1, t2, t3):
        pl.semaphore_signal(
            barrier, inc=1, device_id={"tp": other}, device_id_type=pl.DeviceIdType.MESH
        )
    pl.semaphore_signal(
        barrier, inc=1, device_id={"fs": across}, device_id_type=pl.DeviceIdType.MESH
    )

    @pl.when(has_above)
    def _():
        pl.semaphore_signal(
            barrier, inc=1, device_id={"fs": above}, device_id_type=pl.DeviceIdType.MESH
        )

    @pl.when(has_below)
    def _():
        pl.semaphore_signal(
            barrier, inc=1, device_id={"fs": below}, device_id_type=pl.DeviceIdType.MESH
        )

    pl.semaphore_wait(
        barrier, 4 + has_above.astype(jnp.int32) + has_below.astype(jnp.int32)
    )

    def up_piece(line, column, u):
        row = (line * 2 + column) * up_rows + u * ucut
        return up.at[pl.ds(pl.multiple_of(row, ucut), ucut), :]

    def up_copy(way, line, u, to):
        piece = up_piece(line, y, u)
        recv = upy_recv if way == 2 else upz_recv
        return remote(piece, piece, up_send.at[way, line, u], recv.at[line, u], fs=to)

    def up_onward(line, u, start):
        def go(copy):
            copy.start() if start else copy.wait_send()

        @pl.when(has_above & (line <= z))
        def _():
            go(up_copy(0, line, u, above))

        @pl.when(has_below & (line >= z))
        def _():
            go(up_copy(1, line, u, below))

        go(up_copy(2, line, u, across))

    for u in range(UP_CUTS):
        up_onward(z, u, True)

    def gather_copy(column, to):
        return remote(
            shard, down_block(f, column), gather_send.at[0], gather_recv.at[column], tp=to
        )

    @pl.when(owner != t)
    def _():
        gather_copy(t, owner).start()

    load.wait()

    def tok_copy(way, column, to):
        piece = tok.at[:, pl.ds(pl.multiple_of(column * feats, feats), feats)]
        return remote(piece, piece, tok_send.at[way], tok_recv.at[way], tp=to)

    tok_copy(1, t, t2).start()
    tok_copy(0, t, t1).start()

    @pl.loop(1, lines)
    def _(d):
        for u in range(UP_CUTS):
            @pl.when(z - d >= 0)
            def _():
                up_copy(0, z - d, u, above).wait_recv()
                up_onward(z - d, u, True)

            @pl.when(z + d < lines)
            def _():
                up_copy(1, z + d, u, below).wait_recv()
                up_onward(z + d, u, True)

    tok_copy(1, t2, t2).wait_recv()
    tok_copy(2, t2, t1).start()

    order = (t2, t3, t1, t)

    def down_piece(column, js, side, q):
        line = t * starts + js
        row = ((line * 2 + side) % members) * down_rows + q * dcut
        return down.at[
            pl.ds(pl.multiple_of(row, dcut), dcut),
            pl.ds(pl.multiple_of(column * feats, feats), feats),
        ]

    def down_copy(way, ci, js, q, to):
        piece = down_piece(order[ci], js, y, q)
        recv = downy_recv if way == 2 else downz_recv
        return remote(
            piece, piece, down_send.at[way, ci, js, q], recv.at[ci, js, q], fs=to
        )

    def down_onward(ci, js, q, start):
        line = t * starts + js

        def go(copy):
            copy.start() if start else copy.wait_send()

        @pl.when(has_above & (line <= z))
        def _():
            go(down_copy(0, ci, js, q, above))

        @pl.when(has_below & (line >= z))
        def _():
            go(down_copy(1, ci, js, q, below))

        go(down_copy(2, ci, js, q, across))

    def relay(ci, q):
        @pl.loop(0, starts)
        def _(js):
            line = t * starts + js

            if q == 0 and ci < 3:
                @pl.when(line == z)
                def _():
                    gather_copy(order[ci], t).wait_recv()

            @pl.when(line != z)
            def _():
                down_copy(0, ci, js, q, above).wait_recv()

            down_onward(ci, js, q, True)

    def relayed(ci):
        @pl.loop(0, starts)
        def _(js):
            for q in range(DOWN_CUTS):
                piece = down_piece(order[ci], js, 1 - y, q)
                remote(
                    piece, piece, down_send.at[2, ci, js, q], downy_recv.at[ci, js, q],
                    fs=across,
                ).wait_recv()

    for q in range(DOWN_CUTS):
        relay(0, q)

    tok_copy(0, t1, t1).wait_recv()
    tok_copy(2, t3, t1).wait_recv()

    rows_all = tok.shape[0]
    step = min(rows_all, 128)

    @pl.loop(0, rows_all // step)
    def _(i):
        rows = pl.ds(pl.multiple_of(i * step, step), step)
        values = tok[rows, :].astype(f32)
        mean_square = jnp.mean(values * values, axis=-1, keepdims=True)
        scale[rows, :] = lax.rsqrt(mean_square + 1e-06)

    @pl.loop(0, lines)
    def _(line):
        for u in range(UP_CUTS):
            piece = up_piece(line, 1 - y, u)
            remote(
                piece, piece, up_send.at[2, line, u], upy_recv.at[line, u], fs=across
            ).wait_recv()

    up_out = pltpu.make_async_copy(up, upo_ref, local_sem.at[1])
    up_out.start()

    width = up.shape[1]
    tiles = width // COLUMNS
    for q in range(DOWN_CUTS):
        relay(1, q)

        @pl.loop(q * tiles // DOWN_CUTS, (q + 1) * tiles // DOWN_CUTS)
        def _(i):
            columns = pl.ds(pl.multiple_of(i * COLUMNS, COLUMNS), COLUMNS)
            before = jnp.dot(tok[...], up[:, columns], preferred_element_type=f32)
            value = jnp.maximum(before * scale[...], 0.0)
            hidden[:, columns] = (value * value).astype(bf16)

    def product(ci, out):
        @pl.loop(0, feats // COLUMNS)
        def _(i):
            first = pl.multiple_of(order[ci] * feats + i * COLUMNS, COLUMNS)
            out[:, pl.ds(pl.multiple_of(i * COLUMNS, COLUMNS), COLUMNS)] = jnp.dot(
                hidden[...], down[:, pl.ds(first, COLUMNS)], preferred_element_type=f32
            ).astype(out.dtype)

    def pair_copy(i):
        return remote(give.at[i], take.at[i], pair_send.at[i], pair_recv.at[i], tp=t1)

    cross_copy = remote(cross, crossed, cross_send.at[0], cross_recv.at[0], tp=t2)

    relay(2, 0)
    relayed(0)
    product(0, kept)
    for q in range(1, DOWN_CUTS):
        relay(2, q)
    relayed(1)
    product(1, give.at[0])
    pair_copy(0).start()
    relay(3, 0)
    pair_copy(0).wait_recv()
    @pl.loop(0, rows_all // step)
    def _(i):
        rows = pl.ds(pl.multiple_of(i * step, step), step)
        cross[rows, :] = (kept[rows, :].astype(f32) + take[0, rows, :].astype(f32)).astype(bf16)

    cross_copy.start()
    for q in range(1, DOWN_CUTS):
        relay(3, q)
    relayed(2)
    product(2, give.at[1])
    pair_copy(1).start()
    relayed(3)
    down_out = pltpu.make_async_copy(down, downo_ref, local_sem.at[2])
    down_out.start()
    product(3, own)
    pair_copy(1).wait_recv()
    cross_copy.wait_recv()

    @pl.loop(0, rows_all // step)
    def _(i):
        rows = pl.ds(pl.multiple_of(i * step, step), step)
        mixed_ref[rows, :] = (
            own[rows, :] + take[1, rows, :].astype(f32) + crossed[rows, :].astype(f32)
        ).astype(bf16)

    @pl.loop(0, lines)
    def _(line):
        for u in range(UP_CUTS):
            up_onward(line, u, False)

    @pl.loop(0, starts)
    def _(js):
        for ci in range(4):
            for q in range(DOWN_CUTS):
                down_onward(ci, js, q, False)

    @pl.when(owner != t)
    def _():
        gather_copy(t, owner).wait_send()

    tok_copy(0, t, t1).wait_send()
    tok_copy(1, t, t2).wait_send()
    tok_copy(2, t2, t1).wait_send()
    pair_copy(0).wait_send()
    pair_copy(1).wait_send()
    cross_copy.wait_send()
    up_out.wait()
    down_out.wait()


def fused(n, n_tp, tokens, norm_gain, up_master, down_master):
    rows, feats = tokens.shape
    up_rows, width = up_master.shape
    down_rows = down_master.shape[0]
    depth = up_rows * n
    model = feats * n_tp
    lines, starts = n // 2, n // n_tp // 2
    bf16, f32 = jnp.bfloat16, jnp.float32
    dma = pltpu.SemaphoreType.DMA
    vmem = pl.BlockSpec(memory_space=pltpu.VMEM)
    hbm = pl.BlockSpec(memory_space=pl.ANY)
    flops = 4 * rows * depth * width
    return pl.pallas_call(
        functools.partial(kernel, n, n_tp),
        out_shape=(
            jax.ShapeDtypeStruct((rows, feats), bf16),
            jax.ShapeDtypeStruct((depth, width), bf16),
            jax.ShapeDtypeStruct((width, model), bf16),
        ),
        in_specs=[hbm, vmem, vmem, vmem],
        out_specs=(vmem, hbm, hbm),
        scratch_shapes=[
            pltpu.VMEM((rows, model), bf16),
            pltpu.VMEM((depth, width), bf16),
            pltpu.VMEM((width, model), bf16),
            pltpu.VMEM((down_rows, feats), bf16),
            pltpu.VMEM((rows, 1), f32),
            pltpu.VMEM((rows, width), bf16),
            pltpu.VMEM((rows, feats), f32),
            pltpu.VMEM((2, rows, feats), bf16),
            pltpu.VMEM((2, rows, feats), bf16),
            pltpu.VMEM((rows, feats), bf16),
            pltpu.VMEM((rows, feats), bf16),
            pltpu.VMEM((rows, feats), f32),
            dma((3,)), dma((3,)), dma((1,)), dma((n_tp,)),
            dma((3, lines, UP_CUTS)), dma((lines, UP_CUTS)), dma((lines, UP_CUTS)),
            dma((3, 4, starts, DOWN_CUTS)),
            dma((4, starts, DOWN_CUTS)), dma((4, starts, DOWN_CUTS)),
            dma((2,)), dma((2,)), dma((1,)), dma((1,)), dma((3,)),
        ],
        compiler_params=pltpu.CompilerParams(
            collective_id=0, has_side_effects=True, vmem_limit_bytes=56 * MIB
        ),
        cost_estimate=pl.CostEstimate(flops=flops, bytes_accessed=16 * MIB, transcendentals=0),
        name="layer",
    )(tokens, norm_gain[:, None], up_master, down_master)


def solution(mesh):
    n, n_tp = mesh.shape["fs"], mesh.shape["tp"]
    return jax.shard_map(
        functools.partial(fused, n, n_tp),
        mesh=mesh,
        in_specs=(P("fs", "tp"), P("fs"), P("fs", "tp"), P("fs", "tp")),
        out_specs=(P("fs", "tp"), P(None, "tp"), P("tp", None)),
        check_vma=False,
    )
```

time: 288 us -> 127 us (0.44)
  waiting for transfers between devices: 230 us -> 0 us
  Pallas kernels: 0 us -> 115 us
  matrix products: 14.7 us -> 0 us
  between operations: 13.8 us -> 0.64 us
  other arithmetic: 7.31 us -> 0 us
  local copies, waits for them, and re-layouts: 17.3 us -> 10.6 us
  starting transfers between devices: 5.06 us -> 0 us
    all_gather x3 -> x0, waiting for transfers between devices: 177 us -> none  [the longest x1 73.9 us: shards(): gathered = lax.all_gather(down_local, 'fs', axis=0, tiled=True)]
    pallas_call x0 -> x1, Pallas kernels: none -> 115 us  [fused(): pl.pallas_call(functools.partial(kernel, n, n_tp), out_shape=(jax.ShapeDt...]
    reduce_scatter x1 -> x0, waiting for transfers between devices: 36.6 us -> none  [shards(): lax.psum_scatter(partial_value.astype(jnp.bfloat16), 'tp', scatter_dimens...]
    all_to_all x1 -> x0, waiting for transfers between devices: 15.3 us -> none  [shards(): lax.all_to_all(gathered, 'tp', split_axis=0, concat_axis=1, tiled=True)]
    dot_general x1 -> x0, matrix products: 14.7 us -> none  [shards(): jnp.dot(hidden, down_ready, preferred_element_type=jnp.float32)]
    all_to_all x1 -> x0, local copies, waits for them, and re-layouts: 6.21 us -> none  [shards(): lax.all_to_all(gathered, 'tp', split_axis=0, concat_axis=1, tiled=True)]
    all_to_all x1 -> x0, starting transfers between devices: 4.9 us -> none  [shards(): lax.all_to_all(gathered, 'tp', split_axis=0, concat_axis=1, tiled=True)]
    convert_element_type x2 -> x0, other arithmetic: 4.23 us -> none  [the longest x1 2.15 us: shards(): up_local = (norm_gain[:, None] * up_master).astype(jnp.bfloat16)]
  transfers between devices with their start and end apart: 5 -> 0, of which waited for: 5 -> 0; matrix products, arithmetic and copies ran while one was open for 6% -> 0% of each run, Pallas kernels for 0% -> 0%
where the time goes in v1:
time: 127 us
  Pallas kernels  115 us (91%)
  local copies, waits for them, and re-layouts  10.6 us (8%)
    pallas_call x1, Pallas kernels, fused(): pl.pallas_call(functools.partial(kernel, n, n_tp), out_shape=(jax.ShapeDt...  115 us
    unnamed x5, local copies, waits for them, and re-layouts  9.09 us

profile of v1, /device:TPU:0, one launch (start us, length us, event | category | flops | bytes accessed | tf_op | source)
XLA Modules:
  0.0 126.7 jit_solution(11415997525617304566)
XLA Ops:
  0.6 1.5 %copy.7.gain_ref = f32[256,1]{1,0:T(8,128)} copy(f32[256,1]{0,1:T(1,128)} %bitcast.1) | data formatting | bytes 2048 | tf_op jit(solution)/shard_map/broadcast_in_dim | solution.py:371
  2.1 115.5 %layer.1 = (bf16[1024,512]{1,0:T(8,128)(2,1)}, bf16[2048,1024]{1,0:T(8,128)(2,1)}, bf16[1024,2048]{1,0:T(8,128)(2,1)}) custom-call(bf16[1024,512]{1,0:T(8,128)(2,1)} %tokens_ref.1, f32[256,1]{1,0:T(8,128)} %copy.7.gain_ref, f32[256,1024]{1,0:T(8,128)} %upm_ref.1, f32[512,512]{1,0:T(8,128)} %downm_ref.1), custom_call_target="tpu_custom_call" | custom-call | flops 8589934592 | bytes 16777216 | tf_op jit(solution)/shard_map/layer/pallas_call | solution.py:338
  117.6 2.3 %copy.11 = bf16[1024,512]{1,0:T(8,128)(2,1)} copy(bf16[1024,512]{1,0:T(8,128)(2,1)} %get-tuple-element.6) | data formatting | bytes 2097152
  119.8 0.0 copy-start
  119.8 4.8 %copy.12 = bf16[2048,1024]{1,0:T(8,128)(2,1)} copy(bf16[2048,1024]{1,0:T(8,128)(2,1)} %get-tuple-element.7) | data formatting | bytes 8388608
  124.7 0.0 copy-done
  124.7 2.0 %copy.13 = bf16[1024,2048]{1,0:T(8,128)(2,1)} copy(bf16[1024,2048]{1,0:T(8,128)(2,1)S(1)} %copy-done) | data formatting | bytes 8388608
Async XLA Ops:
  119.8 4.8 %copy-start = (bf16[1024,2048]{1,0:T(8,128)(2,1)S(1)}, bf16[1024,2048]{1,0:T(8,128)(2,1)}, u32[]{:S(2)}) copy-start(bf16[1024,2048]{1,0:T(8,128)(2,1)} %get-tuple-element.8) | copy-start | bytes 12582916

commit v2 on v1

--- a/solution.py
+++ b/solution.py
@@ -8,16 +8,18 @@
 from jax.sharding import PartitionSpec as P
 
 UP_CUTS = 2
-DOWN_CUTS = 4
+DOWN_CUTS = 2
 COLUMNS = 256
+LANES = 128
+VMEM_LIMIT = 40
 MIB = 1024 * 1024
 
 
 def kernel(
     n, n_tp,
     tokens_ref, gain_ref, upm_ref, downm_ref,
-    mixed_ref, upo_ref, downo_ref,
-    tok, up, down, shard, scale, hidden, kept, give, take, cross, crossed, own,
+    mixed_ref, up, down,
+    tok, shard, scale, hidden, kept, give, take, cross, crossed, own,
     tok_send, tok_recv, gather_send, gather_recv,
     up_send, upz_recv, upy_recv,
     down_send, downz_recv, downy_recv,
@@ -63,9 +65,11 @@
     def _():
         down_block(f, t)[...] = downm_ref[...].astype(bf16)
 
-    up[pl.ds(pl.multiple_of(f * up_rows, up_rows), up_rows), :] = (
-        gain_ref[...] * upm_ref[...]
-    ).astype(bf16)
+    gain = jnp.transpose(jnp.broadcast_to(gain_ref[...], (LANES, up_rows)))
+    for first in range(0, up.shape[1], LANES):
+        up[pl.ds(pl.multiple_of(f * up_rows, up_rows), up_rows), pl.ds(first, LANES)] = (
+            gain * upm_ref[:, pl.ds(first, LANES)]
+        ).astype(bf16)
 
     barrier = pltpu.get_barrier_semaphore()
     for other in (t1, t2, t3):
@@ -152,18 +156,20 @@
     tok_copy(1, t2, t2).wait_recv()
     tok_copy(2, t2, t1).start()
 
-    order = (t2, t3, t1, t)
-
-    def down_piece(column, js, side, q):
+    half = feats // 2
+    order = ((t2, 0), (t3, 0), (t2, 1), (t3, 1), (t1, 0), (t1, 1), (t, 0), (t, 1))
+
+    def down_piece(ci, js, side, q):
+        column, part = order[ci]
         line = t * starts + js
         row = ((line * 2 + side) % members) * down_rows + q * dcut
         return down.at[
             pl.ds(pl.multiple_of(row, dcut), dcut),
-            pl.ds(pl.multiple_of(column * feats, feats), feats),
+            pl.ds(pl.multiple_of(column * feats + part * half, half), half),
         ]
 
     def down_copy(way, ci, js, q, to):
-        piece = down_piece(order[ci], js, y, q)
+        piece = down_piece(ci, js, y, q)
         recv = downy_recv if way == 2 else downz_recv
         return remote(
             piece, piece, down_send.at[way, ci, js, q], recv.at[ci, js, q], fs=to
@@ -190,10 +196,10 @@
         def _(js):
             line = t * starts + js
 
-            if q == 0 and ci < 3:
+            if q == 0 and ci in (0, 1, 4):
                 @pl.when(line == z)
                 def _():
-                    gather_copy(order[ci], t).wait_recv()
+                    gather_copy(order[ci][0], t).wait_recv()
 
             @pl.when(line != z)
             def _():
@@ -205,14 +211,15 @@
         @pl.loop(0, starts)
         def _(js):
             for q in range(DOWN_CUTS):
-                piece = down_piece(order[ci], js, 1 - y, q)
+                piece = down_piece(ci, js, 1 - y, q)
                 remote(
                     piece, piece, down_send.at[2, ci, js, q], downy_recv.at[ci, js, q],
                     fs=across,
                 ).wait_recv()
 
-    for q in range(DOWN_CUTS):
-        relay(0, q)
+    for ci in (0, 1):
+        for q in range(DOWN_CUTS):
+            relay(ci, q)
 
     tok_copy(0, t1, t1).wait_recv()
     tok_copy(2, t3, t1).wait_recv()
@@ -235,13 +242,10 @@
                 piece, piece, up_send.at[2, line, u], upy_recv.at[line, u], fs=across
             ).wait_recv()
 
-    up_out = pltpu.make_async_copy(up, upo_ref, local_sem.at[1])
-    up_out.start()
-
     width = up.shape[1]
     tiles = width // COLUMNS
     for q in range(DOWN_CUTS):
-        relay(1, q)
+        relay(2, q)
 
         @pl.loop(q * tiles // DOWN_CUTS, (q + 1) * tiles // DOWN_CUTS)
         def _(i):
@@ -250,53 +254,71 @@
             value = jnp.maximum(before * scale[...], 0.0)
             hidden[:, columns] = (value * value).astype(bf16)
 
-    def product(ci, out):
-        @pl.loop(0, feats // COLUMNS)
-        def _(i):
-            first = pl.multiple_of(order[ci] * feats + i * COLUMNS, COLUMNS)
-            out[:, pl.ds(pl.multiple_of(i * COLUMNS, COLUMNS), COLUMNS)] = jnp.dot(
-                hidden[...], down[:, pl.ds(first, COLUMNS)], preferred_element_type=f32
-            ).astype(out.dtype)
+    def product(ci):
+        column, part = order[ci]
+        first = pl.multiple_of(column * feats + part * half, half)
+        return jnp.dot(hidden[...], down[:, pl.ds(first, half)], preferred_element_type=f32)
 
     def pair_copy(i):
         return remote(give.at[i], take.at[i], pair_send.at[i], pair_recv.at[i], tp=t1)
 
-    cross_copy = remote(cross, crossed, cross_send.at[0], cross_recv.at[0], tp=t2)
-
-    relay(2, 0)
+    def cross_copy(i):
+        return remote(
+            cross.at[i], crossed.at[i], cross_send.at[i], cross_recv.at[i], tp=t2
+        )
+
+    def cross_over(i):
+        pair_copy(i).wait_recv()
+
+        @pl.loop(0, rows_all // step)
+        def _(j):
+            rows = pl.ds(pl.multiple_of(j * step, step), step)
+            cross[i, rows, :] = (kept[rows, :] + take[i, rows, :].astype(f32)).astype(bf16)
+
+        cross_copy(i).start()
+
+    relay(3, 0)
     relayed(0)
-    product(0, kept)
-    for q in range(1, DOWN_CUTS):
-        relay(2, q)
-    relayed(1)
-    product(1, give.at[0])
-    pair_copy(0).start()
-    relay(3, 0)
-    pair_copy(0).wait_recv()
-    @pl.loop(0, rows_all // step)
-    def _(i):
-        rows = pl.ds(pl.multiple_of(i * step, step), step)
-        cross[rows, :] = (kept[rows, :].astype(f32) + take[0, rows, :].astype(f32)).astype(bf16)
-
-    cross_copy.start()
+    kept[...] = product(0)
     for q in range(1, DOWN_CUTS):
         relay(3, q)
+    relayed(1)
+    give[0] = product(1).astype(bf16)
+    pair_copy(0).start()
+    relay(4, 0)
+    cross_over(0)
+    for q in range(1, DOWN_CUTS):
+        relay(4, q)
     relayed(2)
-    product(2, give.at[1])
+    kept[...] = product(2)
+    for q in range(DOWN_CUTS):
+        relay(5, q)
+    relayed(3)
+    give[1] = product(3).astype(bf16)
     pair_copy(1).start()
-    relayed(3)
-    down_out = pltpu.make_async_copy(down, downo_ref, local_sem.at[2])
-    down_out.start()
-    product(3, own)
-    pair_copy(1).wait_recv()
-    cross_copy.wait_recv()
-
-    @pl.loop(0, rows_all // step)
-    def _(i):
-        rows = pl.ds(pl.multiple_of(i * step, step), step)
-        mixed_ref[rows, :] = (
-            own[rows, :] + take[1, rows, :].astype(f32) + crossed[rows, :].astype(f32)
-        ).astype(bf16)
+    relay(6, 0)
+    cross_over(1)
+    for q in range(1, DOWN_CUTS):
+        relay(6, q)
+    for q in range(DOWN_CUTS):
+        relay(7, q)
+    for ci, i in ((4, 2), (5, 3)):
+        relayed(ci)
+        give[i] = product(ci).astype(bf16)
+        pair_copy(i).start()
+    for i in range(2):
+        relayed(6 + i)
+        own[...] = product(6 + i)
+        pair_copy(2 + i).wait_recv()
+        cross_copy(i).wait_recv()
+
+        @pl.loop(0, rows_all // step)
+        def _(j):
+            rows = pl.ds(pl.multiple_of(j * step, step), step)
+            mixed_ref[rows, pl.ds(i * half, half)] = (
+                own[rows, :] + take[2 + i, rows, :].astype(f32)
+                + crossed[i, rows, :].astype(f32)
+            ).astype(bf16)
 
     @pl.loop(0, lines)
     def _(line):
@@ -305,7 +327,7 @@
 
     @pl.loop(0, starts)
     def _(js):
-        for ci in range(4):
+        for ci in range(len(order)):
             for q in range(DOWN_CUTS):
                 down_onward(ci, js, q, False)
 
@@ -316,11 +338,10 @@
     tok_copy(0, t, t1).wait_send()
     tok_copy(1, t, t2).wait_send()
     tok_copy(2, t2, t1).wait_send()
-    pair_copy(0).wait_send()
-    pair_copy(1).wait_send()
-    cross_copy.wait_send()
-    up_out.wait()
-    down_out.wait()
+    for i in range(4):
+        pair_copy(i).wait_send()
+    for i in range(2):
+        cross_copy(i).wait_send()
 
 
 def fused(n, n_tp, tokens, norm_gain, up_master, down_master):
@@ -329,6 +350,7 @@
     down_rows = down_master.shape[0]
     depth = up_rows * n
     model = feats * n_tp
+    half = feats // 2
     lines, starts = n // 2, n // n_tp // 2
     bf16, f32 = jnp.bfloat16, jnp.float32
     dma = pltpu.SemaphoreType.DMA
@@ -338,37 +360,35 @@
     return pl.pallas_call(
         functools.partial(kernel, n, n_tp),
         out_shape=(
-            jax.ShapeDtypeStruct((rows, feats), bf16),
-            jax.ShapeDtypeStruct((depth, width), bf16),
-            jax.ShapeDtypeStruct((width, model), bf16),
+            pltpu.VMEM((rows, feats), bf16),
+            pltpu.VMEM((depth, width), bf16),
+            pltpu.VMEM((width, model), bf16),
         ),
         in_specs=[hbm, vmem, vmem, vmem],
-        out_specs=(vmem, hbm, hbm),
+        out_specs=(vmem, vmem, vmem),
         scratch_shapes=[
             pltpu.VMEM((rows, model), bf16),
-            pltpu.VMEM((depth, width), bf16),
-            pltpu.VMEM((width, model), bf16),
             pltpu.VMEM((down_rows, feats), bf16),
             pltpu.VMEM((rows, 1), f32),
             pltpu.VMEM((rows, width), bf16),
-            pltpu.VMEM((rows, feats), f32),
-            pltpu.VMEM((2, rows, feats), bf16),
-            pltpu.VMEM((2, rows, feats), bf16),
-            pltpu.VMEM((rows, feats), bf16),
-            pltpu.VMEM((rows, feats), bf16),
-            pltpu.VMEM((rows, feats), f32),
+            pltpu.VMEM((rows, half), f32),
+            pltpu.VMEM((4, rows, half), bf16),
+            pltpu.VMEM((4, rows, half), bf16),
+            pltpu.VMEM((2, rows, half), bf16),
+            pltpu.VMEM((2, rows, half), bf16),
+            pltpu.VMEM((rows, half), f32),
             dma((3,)), dma((3,)), dma((1,)), dma((n_tp,)),
             dma((3, lines, UP_CUTS)), dma((lines, UP_CUTS)), dma((lines, UP_CUTS)),
-            dma((3, 4, starts, DOWN_CUTS)),
-            dma((4, starts, DOWN_CUTS)), dma((4, starts, DOWN_CUTS)),
-            dma((2,)), dma((2,)), dma((1,)), dma((1,)), dma((3,)),
+            dma((3, 8, starts, DOWN_CUTS)),
+            dma((8, starts, DOWN_CUTS)), dma((8, starts, DOWN_CUTS)),
+            dma((4,)), dma((4,)), dma((2,)), dma((2,)), dma((1,)),
         ],
         compiler_params=pltpu.CompilerParams(
-            collective_id=0, has_side_effects=True, vmem_limit_bytes=56 * MIB
+            collective_id=0, has_side_effects=True, vmem_limit_bytes=VMEM_LIMIT * MIB
         ),
         cost_estimate=pl.CostEstimate(flops=flops, bytes_accessed=16 * MIB, transcendentals=0),
         name="layer",
-    )(tokens, norm_gain[:, None], up_master, down_master)
+    )(tokens, norm_gain[None, :], up_master, down_master)
 
 
 def solution(mesh):

time: 127 us -> 112 us (0.88)
  Pallas kernels: 115 us -> 102 us
    pallas_call x1, Pallas kernels: 115 us -> 102 us  [fused(): pl.pallas_call(functools.partial(kernel, n, n_tp), out_shape=(pltpu.VMEM(...]
    broadcast_in_dim x1 -> x0, local copies, waits for them, and re-layouts: 1.47 us -> none  [fused(): norm_gain[:, None]]
    unnamed x5 -> x11, local copies, waits for them, and re-layouts: 9.09 us -> 9.34 us
where the time goes in v2:
time: 112 us
  Pallas kernels  102 us (91%)
  local copies, waits for them, and re-layouts  9.34 us (8%)
    pallas_call x1, Pallas kernels, fused(): pl.pallas_call(functools.partial(kernel, n, n_tp), out_shape=(pltpu.VMEM(...  102 us
    unnamed x11, local copies, waits for them, and re-layouts  9.34 us

profile of v2, /device:TPU:0, one launch (start us, length us, event | category | flops | bytes accessed | tf_op | source)
XLA Modules:
  0.0 112.1 jit_solution(7413244800995231038)
XLA Ops:
  0.6 0.0 copy-start
  0.6 1.2 %copy-done = bf16[1024,512]{1,0:T(8,128)(2,1)S(1)} copy-done((bf16[1024,512]{1,0:T(8,128)(2,1)S(1)}, bf16[1024,512]{1,0:T(8,128)(2,1)}, u32[]{:S(2)}) %copy-start) | copy-done | bytes 1048600
  1.9 0.0 copy-start.1
  1.9 1.2 %copy-done.1 = f32[256,1024]{1,0:T(8,128)S(1)} copy-done((f32[256,1024]{1,0:T(8,128)S(1)}, f32[256,1024]{1,0:T(8,128)}, u32[]{:S(2)}) %copy-start.1) | copy-done | bytes 1048600
  3.1 0.0 copy-start.2
  3.1 1.2 %copy-done.2 = f32[512,512]{1,0:T(8,128)S(1)} copy-done((f32[512,512]{1,0:T(8,128)S(1)}, f32[512,512]{1,0:T(8,128)}, u32[]{:S(2)}) %copy-start.2) | copy-done | bytes 1048600
  4.3 0.0 copy-start.3
  4.3 0.7 copy-done.3
  5.0 102.1 %layer.1 = (bf16[1024,512]{1,0:T(8,128)(2,1)S(1)}, bf16[2048,1024]{1,0:T(8,128)(2,1)S(1)}, bf16[1024,2048]{1,0:T(8,128)(2,1)S(1)}) custom-call(bf16[1024,512]{1,0:T(8,128)(2,1)S(1)} %copy-done, f32[1,256]{1,0:T(1,128)S(1)} %bitcast.1, f32[256,1024]{1,0:T(8,128)S(1)} %copy-done.1, f32[512,512]{1,0:T(8,128)S(1)} %copy-done.2), custom_call_target="tpu_custom_call" | custom-call | flops 8589934592 | bytes 16777216 | tf_op jit(solution)/shard_map/layer/pallas_call | solution.py:360
  107.1 1.0 copy.10
  108.0 2.0 %copy.11 = bf16[2048,1024]{1,0:T(8,128)(2,1)} copy(bf16[2048,1024]{1,0:T(8,128)(2,1)S(1)} %get-tuple-element.4) | data formatting | bytes 8388608
  110.1 2.0 %copy.12 = bf16[1024,2048]{1,0:T(8,128)(2,1)} copy(bf16[1024,2048]{1,0:T(8,128)(2,1)S(1)} %get-tuple-element.5) | data formatting | bytes 8388608
Async XLA Ops:
  0.6 1.2 %copy-start = (bf16[1024,512]{1,0:T(8,128)(2,1)S(1)}, bf16[1024,512]{1,0:T(8,128)(2,1)}, u32[]{:S(2)}) copy-start(bf16[1024,512]{1,0:T(8,128)(2,1)} %tokens_ref.1) | copy-start | bytes 3145732
  1.9 1.2 %copy-start.1 = (f32[256,1024]{1,0:T(8,128)S(1)}, f32[256,1024]{1,0:T(8,128)}, u32[]{:S(2)}) copy-start(f32[256,1024]{1,0:T(8,128)} %upm_ref.1) | copy-start | bytes 3145732
  3.1 1.2 %copy-start.2 = (f32[512,512]{1,0:T(8,128)S(1)}, f32[512,512]{1,0:T(8,128)}, u32[]{:S(2)}) copy-start(f32[512,512]{1,0:T(8,128)} %downm_ref.1) | copy-start | bytes 3145732
  4.3 0.7 copy-start.3

commit v3 on v2

--- a/solution.py
+++ b/solution.py
@@ -17,11 +17,11 @@
 
 def kernel(
     n, n_tp,
-    tokens_ref, gain_ref, upm_ref, downm_ref,
-    mixed_ref, up, down,
-    tok, shard, scale, hidden, kept, give, take, cross, crossed, own,
+    tokens_hbm, gain_hbm, upm_hbm, downm_hbm,
+    up, down, own, take, crossed,
+    gain_in, upm_in, downm_in, tok, shard, scale, hidden, kept, give, cross,
     tok_send, tok_recv, gather_send, gather_recv,
-    up_send, upz_recv, upy_recv,
+    up_send, upz_recv, upy_recv, both_send, both_recv,
     down_send, downz_recv, downy_recv,
     pair_send, pair_recv, cross_send, cross_recv, local_sem,
 ):
@@ -39,10 +39,12 @@
     across = f + 1 - 2 * y
     has_above, has_below = z < lines - 1, z > 0
 
-    up_rows = upm_ref.shape[0]
-    down_rows = downm_ref.shape[0]
-    feats = tokens_ref.shape[1]
-    ucut, dcut = up_rows // UP_CUTS, down_rows // DOWN_CUTS
+    up_rows = upm_in.shape[0]
+    down_rows = downm_in.shape[0]
+    feats = tokens_hbm.shape[1]
+    dcut = down_rows // DOWN_CUTS
+    first_cut = max(8, up_rows // 8)
+    ucuts = (first_cut, first_cut + (up_rows - first_cut) // 16 * 8, up_rows)
 
     def remote(src, dst, send, recv, **to):
         return pltpu.make_async_remote_copy(
@@ -50,26 +52,21 @@
             device_id=to, device_id_type=pl.DeviceIdType.MESH,
         )
 
-    load = pltpu.make_async_copy(
-        tokens_ref, tok.at[:, pl.ds(pl.multiple_of(t * feats, feats), feats)], local_sem.at[0]
-    )
-    load.start()
-
-    shard[...] = downm_ref[...].astype(bf16)
-
     def down_block(source, column):
         rows = pl.ds(pl.multiple_of(source % members * down_rows, down_rows), down_rows)
         return down.at[rows, pl.ds(pl.multiple_of(column * feats, feats), feats)]
 
-    @pl.when(owner == t)
-    def _():
-        down_block(f, t)[...] = downm_ref[...].astype(bf16)
-
-    gain = jnp.transpose(jnp.broadcast_to(gain_ref[...], (LANES, up_rows)))
-    for first in range(0, up.shape[1], LANES):
-        up[pl.ds(pl.multiple_of(f * up_rows, up_rows), up_rows), pl.ds(first, LANES)] = (
-            gain * upm_ref[:, pl.ds(first, LANES)]
-        ).astype(bf16)
+    loads = [
+        pltpu.make_async_copy(upm_hbm, upm_in, local_sem.at[0]),
+        pltpu.make_async_copy(gain_hbm, gain_in, local_sem.at[1]),
+        pltpu.make_async_copy(downm_hbm, downm_in, local_sem.at[2]),
+        pltpu.make_async_copy(
+            tokens_hbm, tok.at[:, pl.ds(pl.multiple_of(t * feats, feats), feats)],
+            local_sem.at[3],
+        ),
+    ]
+    for load in loads:
+        load.start()
 
     barrier = pltpu.get_barrier_semaphore()
     for other in (t1, t2, t3):
@@ -92,13 +89,47 @@
             barrier, inc=1, device_id={"fs": below}, device_id_type=pl.DeviceIdType.MESH
         )
 
+    loads[0].wait()
+    loads[1].wait()
+    gain = jnp.transpose(jnp.broadcast_to(gain_in[...], (LANES, up_rows)))
+    for first in range(0, up.shape[1], LANES):
+        up[pl.ds(pl.multiple_of(f * up_rows, up_rows), up_rows), pl.ds(first, LANES)] = (
+            gain * upm_in[:, pl.ds(first, LANES)]
+        ).astype(bf16)
+
+    loads[2].wait()
+    shard[...] = downm_in[...].astype(bf16)
+
+    @pl.when(owner == t)
+    def _():
+        down_block(f, t)[...] = downm_in[...].astype(bf16)
+
     pl.semaphore_wait(
         barrier, 4 + has_above.astype(jnp.int32) + has_below.astype(jnp.int32)
     )
 
     def up_piece(line, column, u):
-        row = (line * 2 + column) * up_rows + u * ucut
-        return up.at[pl.ds(pl.multiple_of(row, ucut), ucut), :]
+        first, last = (ucuts[u], ucuts[u + 1]) if u >= 0 else (0, ucuts[0])
+        row = (line * 2 + column) * up_rows + first
+        return up.at[pl.ds(pl.multiple_of(row, 8), last - first), :]
+
+    def both_copy(way, line, column, to):
+        piece = up_piece(line, column, -1)
+        return remote(
+            piece, piece, both_send.at[way, line, column], both_recv.at[line, column], fs=to
+        )
+
+    def both_onward(line, column, start):
+        def go(copy):
+            copy.start() if start else copy.wait_send()
+
+        @pl.when(has_above & (line <= z))
+        def _():
+            go(both_copy(0, line, column, above))
+
+        @pl.when(has_below & (line >= z))
+        def _():
+            go(both_copy(1, line, column, below))
 
     def up_copy(way, line, u, to):
         piece = up_piece(line, y, u)
@@ -119,6 +150,8 @@
 
         go(up_copy(2, line, u, across))
 
+    both_copy(2, z, y, across).start()
+    both_onward(z, y, True)
     for u in range(UP_CUTS):
         up_onward(z, u, True)
 
@@ -131,7 +164,7 @@
     def _():
         gather_copy(t, owner).start()
 
-    load.wait()
+    loads[3].wait()
 
     def tok_copy(way, column, to):
         piece = tok.at[:, pl.ds(pl.multiple_of(column * feats, feats), feats)]
@@ -140,8 +173,19 @@
     tok_copy(1, t, t2).start()
     tok_copy(0, t, t1).start()
 
+    both_copy(2, z, 1 - y, across).wait_recv()
+    both_onward(z, 1 - y, True)
+
+    def both_relay(line, column):
+        @pl.when((line >= 0) & (line < lines))
+        def _():
+            both_copy(0, line, column, above).wait_recv()
+            both_onward(line, column, True)
+
     @pl.loop(1, lines)
     def _(d):
+        both_relay(z - d, y)
+        both_relay(z + d, y)
         for u in range(UP_CUTS):
             @pl.when(z - d >= 0)
             def _():
@@ -152,6 +196,9 @@
             def _():
                 up_copy(1, z + d, u, below).wait_recv()
                 up_onward(z + d, u, True)
+
+        both_relay(z - d, 1 - y)
+        both_relay(z + d, 1 - y)
 
     tok_copy(1, t2, t2).wait_recv()
     tok_copy(2, t2, t1).start()
@@ -308,22 +355,18 @@
         pair_copy(i).start()
     for i in range(2):
         relayed(6 + i)
-        own[...] = product(6 + i)
+        own[i] = product(6 + i)
         pair_copy(2 + i).wait_recv()
         cross_copy(i).wait_recv()
-
-        @pl.loop(0, rows_all // step)
-        def _(j):
-            rows = pl.ds(pl.multiple_of(j * step, step), step)
-            mixed_ref[rows, pl.ds(i * half, half)] = (
-                own[rows, :] + take[2 + i, rows, :].astype(f32)
-                + crossed[i, rows, :].astype(f32)
-            ).astype(bf16)
 
     @pl.loop(0, lines)
     def _(line):
         for u in range(UP_CUTS):
             up_onward(line, u, False)
+        for column in range(2):
+            both_onward(line, column, False)
+
+    both_copy(2, z, y, across).wait_send()
 
     @pl.loop(0, starts)
     def _(js):
@@ -342,6 +385,30 @@
         pair_copy(i).wait_send()
     for i in range(2):
         cross_copy(i).wait_send()
+
+
+def finish(up, down, own, take, crossed, mixed_hbm, up_hbm, down_hbm, mixed, sems):
+    copies = [
+        pltpu.make_async_copy(up, up_hbm, sems.at[0]),
+        pltpu.make_async_copy(down, down_hbm, sems.at[1]),
+    ]
+    for copy in copies:
+        copy.start()
+    rows_all, half = own.shape[1:]
+    step = min(rows_all, 128)
+    for i in range(2):
+        @pl.loop(0, rows_all // step)
+        def _(j):
+            rows = pl.ds(pl.multiple_of(j * step, step), step)
+            mixed[rows, pl.ds(i * half, half)] = (
+                own[i, rows, :] + take[2 + i, rows, :].astype(jnp.float32)
+                + crossed[i, rows, :].astype(jnp.float32)
+            ).astype(mixed.dtype)
+
+    copies.append(pltpu.make_async_copy(mixed, mixed_hbm, sems.at[2]))
+    copies[2].start()
+    for copy in copies:
+        copy.wait()
 
 
 def fused(n, n_tp, tokens, norm_gain, up_master, down_master):
@@ -355,33 +422,36 @@
     bf16, f32 = jnp.bfloat16, jnp.float32
     dma = pltpu.SemaphoreType.DMA
     vmem = pl.BlockSpec(memory_space=pltpu.VMEM)
-    hbm = pl.BlockSpec(memory_space=pl.ANY)
+    hbm = pl.BlockSpec(memory_space=pltpu.HBM)
     flops = 4 * rows * depth * width
-    return pl.pallas_call(
+    kept = pl.pallas_call(
         functools.partial(kernel, n, n_tp),
         out_shape=(
-            pltpu.VMEM((rows, feats), bf16),
             pltpu.VMEM((depth, width), bf16),
             pltpu.VMEM((width, model), bf16),
+            pltpu.VMEM((2, rows, half), f32),
+            pltpu.VMEM((4, rows, half), bf16),
+            pltpu.VMEM((2, rows, half), bf16),
         ),
-        in_specs=[hbm, vmem, vmem, vmem],
-        out_specs=(vmem, vmem, vmem),
+        in_specs=[hbm] * 4,
+        out_specs=(vmem,) * 5,
         scratch_shapes=[
+            pltpu.VMEM((1, up_rows), f32),
+            pltpu.VMEM(up_master.shape, f32),
+            pltpu.VMEM(down_master.shape, f32),
             pltpu.VMEM((rows, model), bf16),
             pltpu.VMEM((down_rows, feats), bf16),
             pltpu.VMEM((rows, 1), f32),
             pltpu.VMEM((rows, width), bf16),
             pltpu.VMEM((rows, half), f32),
             pltpu.VMEM((4, rows, half), bf16),
-            pltpu.VMEM((4, rows, half), bf16),
             pltpu.VMEM((2, rows, half), bf16),
-            pltpu.VMEM((2, rows, half), bf16),
-            pltpu.VMEM((rows, half), f32),
             dma((3,)), dma((3,)), dma((1,)), dma((n_tp,)),
             dma((3, lines, UP_CUTS)), dma((lines, UP_CUTS)), dma((lines, UP_CUTS)),
+            dma((3, lines, 2)), dma((lines, 2)),
             dma((3, 8, starts, DOWN_CUTS)),
             dma((8, starts, DOWN_CUTS)), dma((8, starts, DOWN_CUTS)),
-            dma((4,)), dma((4,)), dma((2,)), dma((2,)), dma((1,)),
+            dma((4,)), dma((4,)), dma((2,)), dma((2,)), dma((4,)),
         ],
         compiler_params=pltpu.CompilerParams(
             collective_id=0, has_side_effects=True, vmem_limit_bytes=VMEM_LIMIT * MIB
@@ -389,6 +459,19 @@
         cost_estimate=pl.CostEstimate(flops=flops, bytes_accessed=16 * MIB, transcendentals=0),
         name="layer",
     )(tokens, norm_gain[None, :], up_master, down_master)
+    return pl.pallas_call(
+        finish,
+        out_shape=(
+            jax.ShapeDtypeStruct((rows, feats), bf16),
+            jax.ShapeDtypeStruct((depth, width), bf16),
+            jax.ShapeDtypeStruct((width, model), bf16),
+        ),
+        in_specs=[vmem] * 5,
+        out_specs=(hbm,) * 3,
+        scratch_shapes=[pltpu.VMEM((rows, feats), bf16), dma((3,))],
+        compiler_params=pltpu.CompilerParams(vmem_limit_bytes=8 * MIB),
+        name="finish",
+    )(*kept)
 
 
 def solution(mesh):

time: 112 us -> 107 us (0.955)
  local copies, waits for them, and re-layouts: 9.34 us -> 0.67 us
  Pallas kernels: 102 us -> 105 us
    unnamed x11 -> x2, local copies, waits for them, and re-layouts: 9.34 us -> 0.67 us
    pallas_call x0 -> x1, Pallas kernels: none -> 3.64 us  [fused(): pl.pallas_call(finish, out_shape=(jax.ShapeDtypeStruct((rows, feats), bf1...]
where the time goes in v3:
time: 107 us
  Pallas kernels  105 us (98%)
    pallas_call x1, Pallas kernels, fused(): pl.pallas_call(functools.partial(kernel, n, n_tp), out_shape=(pltpu.VMEM(...  102 us
    pallas_call x1, Pallas kernels, fused(): pl.pallas_call(finish, out_shape=(jax.ShapeDtypeStruct((rows, feats), bf1...  3.64 us

profile of v3, /device:TPU:0, one launch (start us, length us, event | category | flops | bytes accessed | tf_op | source)
XLA Modules:
  0.0 106.7 jit_solution(13063210466923664655)
XLA Ops:
  0.6 0.0 copy-start
  0.6 0.7 copy-done
  1.3 101.7 %layer.1 = (bf16[2048,1024]{1,0:T(8,128)(2,1)S(1)}, bf16[1024,2048]{1,0:T(8,128)(2,1)S(1)}, f32[2,1024,256]{2,1,0:T(8,128)S(1)}, bf16[4,1024,256]{2,1,0:T(8,128)(2,1)S(1)}, bf16[2,1024,256]{2,1,0:T(8,128)(2,1)S(1)}) custom-call(bf16[1024,512]{1,0:T(8,128)(2,1)} %tokens_hbm.1, f32[1,256]{1,0:T(1,128)S(1)} %bitcast.1, f32[256,1024]{1,0:T(8,128)} %upm_hbm.1, ...), custom_call_target="tpu_custom_call" | custom-call | flops 8589934592 | bytes 16777216 | tf_op jit(solution)/shard_map/layer/pallas_call | solution.py:427
  103.1 3.6 %finish.1 = (bf16[1024,512]{1,0:T(8,128)(2,1)}, bf16[2048,1024]{1,0:T(8,128)(2,1)}, bf16[1024,2048]{1,0:T(8,128)(2,1)}) custom-call(bf16[2048,1024]{1,0:T(8,128)(2,1)S(1)} %get-tuple-element.8.up, bf16[1024,2048]{1,0:T(8,128)(2,1)S(1)} %get-tuple-element.9.down, f32[2,1024,256]{2,1,0:T(8,128)S(1)} %get-tuple-element.10.own, ...), custom_call_target="tpu_custom_call" | custom-call | tf_op jit(solution)/shard_map/finish/pallas_call | solution.py:462
Async XLA Ops:
  0.6 0.7 copy-start
